TPU v7x, 32 devices: a whole 2x2x4 slice. The times are simulated.
32 devices in a mesh: grp: 2 (over x), sp: 4 (over z), tp: 4 (over y, core).
Axes of the slice: x: 2, y: 2, z: 4, core: 2. Of those that a mesh axis runs over, the one named last changes fastest.
Arguments:
- grid_tokens: bfloat16 [64, 64, 1024], P(('grp', 'sp'), 'tp'), parts along dimension 0, may hold values from -6 to 6
- norm_gain: float32 [2, 1024], replicated, may hold values from 0.1 to 1.9
- w_query: bfloat16 [2, 1024, 512], replicated, may hold values from -0.84375 to 0.84375
- w_key: bfloat16 [2, 1024, 512], replicated, may hold values from -1.1390625 to 1.1390625
- w_value: bfloat16 [2, 1024, 512], replicated, may hold values from -0.1875 to 0.1875
- offset_bias: float32 [2, 4, 15, 31], replicated, may hold values from -5 to 5
- w_out: bfloat16 [2, 512, 1024], replicated, may hold values from -1 to 1
Outputs:
- grid_out: bfloat16 [64, 64, 1024], P(('grp', 'sp'), 'tp'), parts along dimension 0
There are 2 independent parts, one for each index of `grp`. A program takes and returns all parts, laid end to end along the dimension named above; an argument that names none is the same for every part. Nothing has to cross between parts.
All inputs are finite; a program needn't handle non-finite values.
Results may differ from a plain program's by a relative error of at most 0.014.
Values may be sent and summed in bfloat16 or wider, within the bound.
A program may use at most 64 MiB of HBM per device.

v0:
```python
import functools
import math

import jax
import jax.numpy as jnp
from jax import lax
from jax.experimental import pallas as pl
from jax.experimental.pallas import tpu as pltpu
from jax.sharding import PartitionSpec as P

HEAD_DIM = 128
WIN_ROWS = 8
WIN_COLS = 16
NORM_EPSILON = 1e-06
HALF_ROWS = WIN_ROWS // 2
HALF_COLS = WIN_COLS // 2
BELOW = WIN_ROWS - HALF_ROWS - 1
CHUNK_HEADS = 2
MESH = pl.DeviceIdType.MESH
LOG2E = math.log2(math.e)
HIDDEN = -1e30

STEPS = ((1, 0), (-1, 0), (1, 1), (1, -1), (-1, 1), (-1, -1), (0, 1), (0, -1))


def kernel(
    x_hbm, gain_hbm, wq_hbm, wk_hbm, wv_hbm, bias_hbm, wo_hbm, out,
    x, gain, wq, wk, wv, wo, bias, flat, wide, hidden, table, kv, normed, queries, acc,
    local_sem, kv_w_sem, w_sem, send_sem, recv_sem,
    *, sp_count, tp_count,
):
    layers, model_width, inner = wq.shape
    tile_rows, tile_cols, _ = x.shape
    tokens = tile_rows * tile_cols
    heads = inner // HEAD_DIM
    chunks = heads // CHUNK_HEADS
    part = CHUNK_HEADS * HEAD_DIM
    slab_rows = tile_rows + WIN_ROWS
    slab_cols = tile_cols + WIN_COLS
    slab = slab_rows * slab_cols
    own_blocks = tile_cols // HALF_COLS
    row_index = lax.axis_index("sp")
    col_index = lax.axis_index("tp")

    def there(dr, dc):
        r, c = row_index + dr, col_index + dc
        return (r >= 0) & (r < sp_count) & (c >= 0) & (c < tp_count)

    first = [
        pltpu.make_async_copy(x_hbm, x, local_sem.at[0]),
        pltpu.make_async_copy(gain_hbm, gain, local_sem.at[1]),
        pltpu.make_async_copy(bias_hbm, bias, local_sem.at[2]),
    ]
    for copy in first:
        copy.start()
    weight_copies = {}

    def fetch(l, names):
        for name in names:
            if name in "qo":
                src, dst = {"q": (wq_hbm, wq), "o": (wo_hbm, wo)}[name]
                copy = pltpu.make_async_copy(src.at[l], dst.at[l], w_sem.at[l, "qo".index(name)])
                copy.start()
                weight_copies[l, name] = copy
            else:
                src, dst = {"k": (wk_hbm, wk), "v": (wv_hbm, wv)}[name]
                i = "kv".index(name)
                copy = pltpu.make_async_copy(src.at[l], dst.at[l], kv_w_sem.at[l, 0, i])
                copy.start()
                weight_copies[l, 0, i] = copy

    every = ["k", "v"]
    fetch(0, every + ["q"])

    barrier = pltpu.get_barrier_semaphore()
    for dr, dc in STEPS:
        @pl.when(there(dr, dc))
        def _():
            pl.semaphore_signal(
                barrier,
                inc=1,
                device_id={"sp": row_index + dr, "tp": col_index + dc},
                device_id_type=MESH,
            )

    own_rows = slice(HALF_ROWS, HALF_ROWS + tile_rows)
    own_cols = slice(1, 1 + own_blocks)

    def spans(dr, dc):
        if dr == 1:
            rows = slice(tile_rows, tile_rows + HALF_ROWS), slice(0, HALF_ROWS)
        elif dr == -1:
            end = HALF_ROWS + tile_rows
            rows = slice(HALF_ROWS, HALF_ROWS + BELOW), slice(end, end + BELOW)
        else:
            rows = own_rows, own_rows
        if dc == 1:
            cols = slice(own_blocks, own_blocks + 1), slice(0, 1)
        elif dc == -1:
            cols = slice(1, 2), slice(1 + own_blocks, 2 + own_blocks)
        else:
            cols = own_cols, own_cols
        return rows, cols

    def halo_copy(l, g, d):
        dr, dc = STEPS[d]
        (src_rows, dst_rows), (src_cols, dst_cols) = spans(dr, dc)
        return pltpu.make_async_remote_copy(
            src_ref=kv.at[l, g, src_rows, src_cols],
            dst_ref=kv.at[l, g, dst_rows, dst_cols],
            send_sem=send_sem.at[l, g, d],
            recv_sem=recv_sem.at[l, g, d],
            device_id={"sp": row_index + dr, "tp": col_index + dc},
            device_id_type=MESH,
        )

    def fill(rows, cols):
        for l in range(layers):
            for g in range(chunks):
                shape = (rows.stop - rows.start, cols.stop - cols.start) + kv.shape[4:]
                kv[l, g, rows, cols] = jnp.zeros(shape, jnp.bfloat16)

    def zero_missing():
        fill(slice(slab_rows - 1, slab_rows), slice(0, own_blocks + 2))
        for dr, dc in STEPS:
            (_, dst_rows), (_, dst_cols) = spans(dr, dc)

            @pl.when(jnp.logical_not(there(-dr, -dc)))
            def _():
                fill(dst_rows, dst_cols)

    def norm(l, stream):
        factor = lax.rsqrt(jnp.mean(stream * stream, axis=-1, keepdims=True) + NORM_EPSILON)
        normed[...] = (stream * factor * gain[l : l + 1]).astype(jnp.bfloat16)

    def project_kv(l, g):
        cols = slice(g * part, (g + 1) * part)
        for i, w in enumerate((wk, wv)):
            if (l, g, i) in weight_copies:
                weight_copies[l, g, i].wait()
            made = jnp.dot(normed[...], w[l, :, cols], preferred_element_type=jnp.float32)
            made = made.reshape(tile_rows, own_blocks, HALF_COLS, part)
            kv[l, g, own_rows, own_cols, :, i * part : (i + 1) * part] = made.astype(jnp.bfloat16)

    def beside(dc):
        return lax.rem(col_index, 2) == (0 if dc == 1 else 1)

    def relay_copy(l, g, d):
        dr, dc = STEPS[d]
        (_, rows), (src_cols, dst_cols) = spans(dr, dc)
        return pltpu.make_async_remote_copy(
            src_ref=kv.at[l, g, rows, src_cols],
            dst_ref=kv.at[l, g, rows, dst_cols],
            send_sem=send_sem.at[l, g, d],
            recv_sem=recv_sem.at[l, g, d],
            device_id={"sp": row_index, "tp": col_index + dc},
            device_id_type=MESH,
        )

    def direct(dr, dc):
        if dr and dc:
            return there(dr, dc) & jnp.logical_not(beside(dc))
        return there(dr, dc)

    def relayed(dr, dc):
        return there(-dr, 0) & there(0, dc) & beside(dc)

    def send(l, g):
        for d, (dr, dc) in enumerate(STEPS):
            @pl.when(direct(dr, dc))
            def _():
                halo_copy(l, g, d).start()

    def receive_near(l, g):
        for d, (dr, dc) in enumerate(STEPS):
            if dc == 0:
                @pl.when(there(-dr, -dc))
                def _():
                    halo_copy(l, g, d).wait_recv()
        for d, (dr, dc) in enumerate(STEPS):
            if dr and dc:
                @pl.when(relayed(dr, dc))
                def _():
                    relay_copy(l, g, d).start()

    def receive_far(l, g):
        for d, (dr, dc) in enumerate(STEPS):
            if dc:
                @pl.when(there(-dr, -dc))
                def _():
                    halo_copy(l, g, d).wait_recv()

    def project_q(l):
        weight_copies[l, "q"].wait()
        made = jnp.dot(normed[...], wq[l], preferred_element_type=jnp.float32)
        queries[...] = (made * (LOG2E / HEAD_DIM**0.5)).astype(jnp.bfloat16)

    def build_hidden():
        k = lax.broadcasted_iota(jnp.int32, (1, slab), 1)
        key_row = k // slab_cols
        key_col = k - key_row * slab_cols
        row0 = row_index * tile_rows
        col0 = col_index * tile_cols
        c = lax.broadcasted_iota(jnp.int32, (tile_cols, 1), 0)
        col_start = jnp.clip(col0 + c - HALF_COLS, 0, tp_count * tile_cols - WIN_COLS)
        col_start = col_start - (col0 - HALF_COLS)
        col_inside = (key_col >= col_start) & (key_col < col_start + WIN_COLS)
        for r in range(tile_rows):
            start = jnp.clip(row0 + r - HALF_ROWS, 0, sp_count * tile_rows - WIN_ROWS)
            start = start - (row0 - HALF_ROWS)
            row_inside = (key_row >= start) & (key_row < start + WIN_ROWS)
            hidden[r * tile_cols : (r + 1) * tile_cols] = jnp.where(
                col_inside & row_inside, 0.0, HIDDEN
            )

    lead = tile_rows - 1 - BELOW

    def build_flat():
        row_count, col_count = 2 * WIN_ROWS - 1, 2 * WIN_COLS - 1
        flat[...] = jnp.zeros_like(flat)
        for l in range(layers):
            for a in range(row_count):
                place = (lead + a) * slab_cols
                flat[l * heads : (l + 1) * heads, place : place + col_count] = bias[l, a] * LOG2E

    def build_table(l):
        width = flat.shape[1]
        shift = (width - (WIN_COLS - 1 - HALF_COLS)) % width
        for h in range(heads):
            row = l * heads + h
            spread = jnp.broadcast_to(flat[row : row + 1, :], (tile_cols, width))
            wide[...] = pltpu.roll(spread, shift, 1, stride=1, stride_axis=0)
            for r in range(tile_rows):
                first_lane = (tile_rows - 1 - r) * slab_cols
                rows = slice(r * tile_cols, (r + 1) * tile_cols)
                table[l, h, rows] = wide[:, first_lane : first_lane + slab] + hidden[rows]

    def attend(l, g):
        everything = kv[l, g].astype(jnp.float32).reshape(slab, 2 * part).astype(jnp.bfloat16)
        mixed = []
        for i in range(CHUNK_HEADS):
            h = g * CHUNK_HEADS + i
            keys = everything[:, i * HEAD_DIM : (i + 1) * HEAD_DIM]
            values = everything[:, part + i * HEAD_DIM : part + (i + 1) * HEAD_DIM]
            scores = lax.dot_general(
                queries[:, h * HEAD_DIM : (h + 1) * HEAD_DIM], keys,
                (((1,), (1,)), ((), ())), preferred_element_type=jnp.float32,
            ) + table[l, h]
            top = jnp.max(scores, axis=1, keepdims=True)
            expo = jnp.exp2(scores - top)
            total = jnp.sum(expo, axis=1, keepdims=True)
            mix = jnp.dot(expo.astype(jnp.bfloat16), values, preferred_element_type=jnp.float32)
            mixed.append((mix / total).astype(jnp.bfloat16))
        mixture = jnp.concatenate(mixed, axis=1)
        acc[...] += jnp.dot(
            mixture, wo[l, g * part : (g + 1) * part, :], preferred_element_type=jnp.float32
        )

    first[0].wait()
    first[1].wait()
    acc[...] = x[...].reshape(tokens, model_width).astype(jnp.float32)
    for l in range(layers):
        norm(l, acc[...])
        for g in range(chunks):
            project_kv(l, g)
            if l == 0 and g == 0:
                neighbours = sum(
                    jnp.where(there(dr, dc), 1, 0).astype(jnp.int32) for dr, dc in STEPS
                )
                pl.semaphore_wait(barrier, neighbours)
            send(l, g)
        project_q(l)
        if l == 0:
            fetch(0, ["o"])
            for later in range(1, layers):
                fetch(later, every + ["q", "o"])
            zero_missing()
            build_hidden()
            first[2].wait()
            build_flat()
        build_table(l)
        weight_copies[l, "o"].wait()
        receive_near(l, 0)
        for g in range(chunks):
            receive_far(l, g)
            if g + 1 < chunks:
                receive_near(l, g + 1)
            attend(l, g)
        acc[...] = acc[...].astype(jnp.bfloat16).astype(jnp.float32)
    out[...] = acc[...].astype(jnp.bfloat16).reshape(out.shape)
    for l in range(layers):
        for g in range(chunks):
            for d, (dr, dc) in enumerate(STEPS):
                @pl.when(direct(dr, dc))
                def _():
                    halo_copy(l, g, d).wait_send()

                if dr and dc:
                    @pl.when(relayed(dr, dc))
                    def _():
                        relay_copy(l, g, d).wait_send()


def on_device(sp_count, tp_count, grid_tokens, norm_gain, w_query, w_key, w_value, offset_bias, w_out):
    tile_rows, tile_cols, model_width = grid_tokens.shape
    layers, _, inner = w_query.shape
    tokens = tile_rows * tile_cols
    heads = inner // HEAD_DIM
    chunks = heads // CHUNK_HEADS
    part = CHUNK_HEADS * HEAD_DIM
    slab_rows = tile_rows + WIN_ROWS
    slab_cols = tile_cols + WIN_COLS
    slab = slab_rows * slab_cols
    flat_width = -(-(slab + tile_rows * slab_cols) // 128) * 128
    blocks = slab_cols // HALF_COLS
    bias_rows = jnp.transpose(offset_bias, (0, 2, 1, 3))
    bf16, f32 = jnp.bfloat16, jnp.float32
    hbm = pl.BlockSpec(memory_space=pltpu.HBM)
    return pl.pallas_call(
        functools.partial(kernel, sp_count=sp_count, tp_count=tp_count),
        out_shape=jax.ShapeDtypeStruct(grid_tokens.shape, bf16),
        in_specs=[hbm] * 7,
        out_specs=pl.BlockSpec(memory_space=pltpu.VMEM),
        scratch_shapes=[
            pltpu.VMEM(grid_tokens.shape, bf16),
            pltpu.VMEM(norm_gain.shape, f32),
            pltpu.VMEM(w_query.shape, bf16),
            pltpu.VMEM(w_key.shape, bf16),
            pltpu.VMEM(w_value.shape, bf16),
            pltpu.VMEM(w_out.shape, bf16),
            pltpu.VMEM(bias_rows.shape, f32),
            pltpu.VMEM((layers * heads, flat_width), f32),
            pltpu.VMEM((tile_cols, flat_width), f32),
            pltpu.VMEM((tokens, slab), f32),
            pltpu.VMEM((layers, heads, tokens, slab), f32),
            pltpu.VMEM((layers, chunks, slab_rows, blocks, HALF_COLS, 2 * part), bf16),
            pltpu.VMEM((tokens, model_width), bf16),
            pltpu.VMEM((tokens, inner), bf16),
            pltpu.VMEM((tokens, model_width), f32),
            pltpu.SemaphoreType.DMA((4,)),
            pltpu.SemaphoreType.DMA((layers, chunks, 2)),
            pltpu.SemaphoreType.DMA((layers, 2)),
            pltpu.SemaphoreType.DMA((layers, chunks, len(STEPS))),
            pltpu.SemaphoreType.DMA((layers, chunks, len(STEPS))),
        ],
        compiler_params=pltpu.CompilerParams(
            collective_id=0, has_side_effects=True, vmem_limit_bytes=54784 * 1024
        ),
    )(grid_tokens, norm_gain, w_query, w_key, w_value, bias_rows, w_out)


def solution(mesh):
    return jax.shard_map(
        functools.partial(on_device, mesh.shape["sp"], mesh.shape["tp"]),
        mesh=mesh,
        in_specs=(P(("grp", "sp"), "tp", None), P(), P(), P(), P(), P(), P()),
        out_specs=P(("grp", "sp"), "tp", None),
        check_vma=False,
    )
```

profile of v0, /device:TPU:1, one launch (start us, length us, event | category | flops | bytes accessed | tf_op | source)
XLA Modules:
  0.0 20.8 jit_solution(16841192124344329632)
XLA Ops:
  0.0 0.0 copy-start
  0.0 0.8 %copy-done = f32[2,4,15,31]{3,1,2,0:T(4,128)S(1)} copy-done((f32[2,4,15,31]{3,1,2,0:T(4,128)S(1)}, f32[2,4,15,31]{3,1,2,0:T(4,128)}, u32[]{:S(2)}) %copy-start) | copy-done | bytes 14904
  0.8 0.0 copy-start.1
  0.8 0.7 %copy-done.1 = f32[2,1024]{1,0:T(2,128)S(1)} copy-done((f32[2,1024]{1,0:T(2,128)S(1)}, f32[2,1024]{1,0:T(2,128)}, u32[]{:S(2)}) %copy-start.1) | copy-done | bytes 8216
  1.5 18.6 %shard_map.73 = bf16[8,16,1024]{2,1,0:T(8,128)(2,1)S(1)} custom-call(bf16[8,16,1024]{2,1,0:T(8,128)(2,1)} %x_hbm.1, f32[2,1024]{1,0:T(2,128)S(1)} %copy-done.1, bf16[2,1024,512]{2,1,0:T(8,128)(2,1)} %wq_hbm.1, bf16[2,1024,512]{2,1,0:T(8,128)(2,1)} %wk_hbm.1, bf16[2,1024,512]{2,1,0:T(8,128)(2,1)} %wv_hbm.1, f32[2,15,4,31]{3,2,1,0:T(4,128)S(1)} %bitcast.1, ...), custom_call_target="tpu_custom_call" | custom-call | tf_op jit(solution)/shard_map/pallas_call | solution.py:319
  20.1 0.7 %copy.9 = bf16[8,16,1024]{2,1,0:T(8,128)(2,1)} copy(bf16[8,16,1024]{2,1,0:T(8,128)(2,1)S(1)} %shard_map.73) | data formatting | bytes 524288
Async XLA Ops:
  0.0 0.8 %copy-start = (f32[2,4,15,31]{3,1,2,0:T(4,128)S(1)}, f32[2,4,15,31]{3,1,2,0:T(4,128)}, u32[]{:S(2)}) copy-start(f32[2,4,15,31]{3,1,2,0:T(4,128)} %param.12) | copy-start | bytes 44644
  0.8 0.7 %copy-start.1 = (f32[2,1024]{1,0:T(2,128)S(1)}, f32[2,1024]{1,0:T(2,128)}, u32[]{:S(2)}) copy-start(f32[2,1024]{1,0:T(2,128)} %gain_hbm.1) | copy-start | bytes 24580
where the time goes:
time: 21.1 us; the launch traced here: 20.8 us
  Pallas kernels  18.6 us (88%)
  local copies, waits for them, and re-layouts  2.23 us (11%)
    pallas_call x1, Pallas kernels, on_device(): pl.pallas_call(functools.partial(kernel, sp_count=sp_count, tp_count=tp_c...  18.6 us
    unnamed x5, local copies, waits for them, and re-layouts  2.23 us

commit v1 on v0

--- a/solution.py
+++ b/solution.py
@@ -346,7 +346,7 @@
         compiler_params=pltpu.CompilerParams(
             collective_id=0, has_side_effects=True, vmem_limit_bytes=54784 * 1024
         ),
-    )(grid_tokens, norm_gain, w_query, w_key, w_value, bias_rows, w_out)
+    )(grid_tokens, pltpu.with_memory_space_constraint(norm_gain, pltpu.HBM), w_query, w_key, w_value, pltpu.with_memory_space_constraint(bias_rows, pltpu.HBM), w_out)
 
 
 def solution(mesh):

time: 21.1 us -> 19.7 us (0.934)
  local copies, waits for them, and re-layouts: 2.23 us -> 0.71 us
    unnamed x5 -> x1, local copies, waits for them, and re-layouts: 2.23 us -> 0.71 us
where the time goes in v1:
time: 19.7 us; the launch traced here: 19.4 us
  Pallas kernels  18.7 us (95%)
  local copies, waits for them, and re-layouts  0.71 us (4%)
    pallas_call x1, Pallas kernels, on_device(): pl.pallas_call(functools.partial(kernel, sp_count=sp_count, tp_count=tp_c...  18.7 us
    unnamed x1, local copies, waits for them, and re-layouts  0.71 us

profile of v1, /device:TPU:1, one launch (start us, length us, event | category | flops | bytes accessed | tf_op | source)
XLA Modules:
  0.0 19.4 jit_solution(16089301502791622941)
XLA Ops:
  0.0 18.7 %shard_map.73 = bf16[8,16,1024]{2,1,0:T(8,128)(2,1)S(1)} custom-call(bf16[8,16,1024]{2,1,0:T(8,128)(2,1)} %x_hbm.1, f32[2,1024]{1,0:T(2,128)} %gain_hbm.1, bf16[2,1024,512]{2,1,0:T(8,128)(2,1)} %wq_hbm.1, bf16[2,1024,512]{2,1,0:T(8,128)(2,1)} %wk_hbm.1, bf16[2,1024,512]{2,1,0:T(8,128)(2,1)} %wv_hbm.1, f32[2,15,4,31]{3,2,1,0:T(4,128)} %bitcast.1, ...), custom_call_target="tpu_custom_call" | custom-call | tf_op jit(solution)/shard_map/pallas_call | solution.py:319
  18.7 0.7 %copy.9 = bf16[8,16,1024]{2,1,0:T(8,128)(2,1)} copy(bf16[8,16,1024]{2,1,0:T(8,128)(2,1)S(1)} %shard_map.73) | data formatting | bytes 524288

commit v2 on v1

v2 whole, which is shorter than its diff:
```python
import functools
import math

import jax
import jax.numpy as jnp
from jax import lax
from jax.experimental import pallas as pl
from jax.experimental.pallas import tpu as pltpu
from jax.sharding import PartitionSpec as P

HEAD_DIM = 128
WIN_ROWS = 8
WIN_COLS = 16
NORM_EPSILON = 1e-06
HALF_ROWS = WIN_ROWS // 2
HALF_COLS = WIN_COLS // 2
BELOW = WIN_ROWS - HALF_ROWS - 1
MESH = pl.DeviceIdType.MESH
LOG2E = math.log2(math.e)
HIDDEN = -1e30

KINDS = (
    "D_inner", "D_outer", "D_diag", "D_relay", "U_inner", "U_outer", "U_diag", "U_relay",
    "C_beside", "C_far",
)


def kernel(
    x_hbm, gain_hbm, wq_hbm, wk_hbm, wv_hbm, bias_hbm, wo_hbm, out,
    xs, ms, gain, wq, wk, wv, wo, bias, flat, wide, hidden, table, kv, queries, acc, tops, mixes,
    local_sem, w_sem, send_sem, recv_sem,
    *, sp_count, tp_count,
):
    layers, model_width, inner = wq.shape
    tile_rows, own_blocks = x_hbm.shape[:2]
    tile_cols = own_blocks * HALF_COLS
    tokens = tile_rows * tile_cols
    half = HALF_ROWS * tile_cols
    heads = inner // HEAD_DIM
    slab_rows = tile_rows + WIN_ROWS
    slab_cols = tile_cols + WIN_COLS
    slab = slab_rows * slab_cols
    edge = HALF_ROWS * slab_cols
    row_index = lax.axis_index("sp")
    col_index = lax.axis_index("tp")
    side = lax.rem(col_index, 2)
    beside, far = 1 - 2 * side, 2 * side - 1
    inner_block, outer_block = own_blocks - side * (own_blocks - 1), 1 + side * (own_blocks - 1)
    left_block, right_block = side * (own_blocks + 1), (1 - side) * (own_blocks + 1)

    has_above, has_below = row_index > 0, row_index < sp_count - 1
    has_beside = (col_index + beside >= 0) & (col_index + beside < tp_count)
    has_far = (col_index + far >= 0) & (col_index + far < tp_count)
    neighbours = (
        (-1, 0, has_above), (1, 0, has_below), (-1, far, has_above & has_far),
        (1, far, has_below & has_far), (0, far, has_far), (0, beside, has_beside),
    )

    own_rows = slice(HALF_ROWS, HALF_ROWS + tile_rows)
    own_cols = slice(1, 1 + own_blocks)
    every_block = slice(0, own_blocks + 2)
    above_rows = slice(0, HALF_ROWS)
    last_rows = slice(tile_rows, tile_rows + HALF_ROWS)
    first_rows = slice(HALF_ROWS, HALF_ROWS + BELOW)
    below_rows = slice(HALF_ROWS + tile_rows, HALF_ROWS + tile_rows + BELOW)
    OWN = ((own_rows, own_cols),)
    SIDES = ((own_rows, slice(0, 1)), (own_rows, slice(own_blocks + 1, own_blocks + 2)))
    EDGES = (
        (above_rows, every_block), (slice(slab_rows - HALF_ROWS, slab_rows), every_block),
    )

    barrier = pltpu.get_barrier_semaphore()
    for dr, dc, exists in neighbours:
        @pl.when(exists)
        def _():
            pl.semaphore_signal(
                barrier,
                inc=1,
                device_id={"sp": row_index + dr, "tp": col_index + dc},
                device_id_type=MESH,
            )

    first = [
        pltpu.make_async_copy(x_hbm, xs.at[own_rows, own_cols], local_sem.at[0]),
        pltpu.make_async_copy(gain_hbm, gain, local_sem.at[1]),
        pltpu.make_async_copy(bias_hbm, bias, local_sem.at[2]),
    ]
    for copy in first:
        copy.start()
    pairs = {"k": (wk_hbm, wk), "v": (wv_hbm, wv), "q": (wq_hbm, wq), "o": (wo_hbm, wo)}
    weight_copies = {}

    def fetch(l, names):
        for name in names:
            src, dst = pairs[name]
            copy = pltpu.make_async_copy(src.at[l], dst.at[l], w_sem.at[l, "kvqo".index(name)])
            copy.start()
            weight_copies[l, name] = copy

    def arrived(l, name):
        if (l, name) in weight_copies:
            weight_copies.pop((l, name)).wait()

    fetch(0, "kvq")

    def plan(kind):
        way, what = kind.split("_")
        if way == "C":
            if what == "beside":
                return own_rows, own_rows, inner_block, left_block, 0, beside, has_beside, has_beside
            return own_rows, own_rows, outer_block, right_block, 0, far, has_far, has_far
        dr = 1 if way == "D" else -1
        src_rows, dst_rows = (last_rows, above_rows) if dr == 1 else (first_rows, below_rows)
        goes, comes = (has_below, has_above) if dr == 1 else (has_above, has_below)
        if what == "inner":
            return src_rows, dst_rows, inner_block, inner_block, dr, 0, goes, comes
        if what == "outer":
            return src_rows, dst_rows, outer_block, outer_block, dr, 0, goes, comes
        if what == "diag":
            ends = outer_block, right_block
            return src_rows, dst_rows, *ends, dr, far, goes & has_far, comes & has_far
        passes = comes & has_beside
        return dst_rows, dst_rows, inner_block, left_block, 0, beside, passes, passes

    def halo_copy(l, kind):
        src_rows, dst_rows, src_block, dst_block, dr, dc, _, _ = plan(kind)
        ref = ms.at[l - 1] if l else xs
        i = KINDS.index(kind)
        return pltpu.make_async_remote_copy(
            src_ref=ref.at[src_rows, pl.ds(src_block, 1)],
            dst_ref=ref.at[dst_rows, pl.ds(dst_block, 1)],
            send_sem=send_sem.at[l, i],
            recv_sem=recv_sem.at[l, i],
            device_id={"sp": row_index + dr, "tp": col_index + dc},
            device_id_type=MESH,
        )

    def send(l, kinds):
        for kind in kinds:
            @pl.when(plan(kind)[6])
            def _():
                halo_copy(l, kind).start()

    def receive(l, kinds):
        for kind in kinds:
            @pl.when(plan(kind)[7])
            def _():
                halo_copy(l, kind).wait_recv()

    def pass_on(l, way):
        receive(l, [way + "_inner"])
        send(l, [way + "_relay"])

    def fill(rows, cols):
        for ref in [xs] + [ms.at[l] for l in range(layers - 1)]:
            shape = (rows.stop - rows.start, cols.stop - cols.start) + ref.shape[2:]
            ref[rows, cols] = jnp.zeros(shape, jnp.bfloat16)

    def zero_missing():
        received = slice(0, slab_rows - 1)
        fill(slice(slab_rows - 1, slab_rows), every_block)

        @pl.when(jnp.logical_not(has_above))
        def _():
            fill(above_rows, every_block)

        @pl.when(jnp.logical_not(has_below))
        def _():
            fill(below_rows, every_block)

        @pl.when(col_index == 0)
        def _():
            fill(received, slice(0, 1))

        @pl.when(col_index == tp_count - 1)
        def _():
            fill(received, slice(own_blocks + 1, own_blocks + 2))

    def gather(ref, pieces):
        width = ref.shape[-1]
        return jnp.concatenate(
            [ref[rows, cols].astype(jnp.float32).reshape(-1, width) for rows, cols in pieces]
        )

    def norm(l, stream):
        factor = lax.rsqrt(jnp.mean(stream * stream, axis=-1, keepdims=True) + NORM_EPSILON)
        return (stream * factor * gain[l : l + 1]).astype(jnp.bfloat16)

    def stream_of(l, pieces):
        stream = gather(xs, pieces)
        for done in range(l):
            mixture = gather(ms.at[done], pieces).astype(jnp.bfloat16)
            stream += jnp.dot(mixture, wo[done], preferred_element_type=jnp.float32)
            stream = stream.astype(jnp.bfloat16).astype(jnp.float32)
        return stream

    def project_kv(l, normed, pieces):
        for i, (name, w) in enumerate((("k", wk), ("v", wv))):
            arrived(l, name)
            made = jnp.dot(normed, w[l], preferred_element_type=jnp.float32)
            place = 0
            for rows, cols in pieces:
                shape = (rows.stop - rows.start, cols.stop - cols.start, HALF_COLS)
                count = math.prod(shape)
                kv[rows, cols, :, i * inner : (i + 1) * inner] = (
                    made[place : place + count].reshape(*shape, inner).astype(jnp.bfloat16)
                )
                place += count

    def project_q(l, normed):
        arrived(l, "q")
        made = jnp.dot(normed, wq[l], preferred_element_type=jnp.float32)
        queries[...] = (made * (LOG2E / HEAD_DIM**0.5)).astype(jnp.bfloat16)

    def prepare_own(l):
        normed = norm(l, acc[...])
        project_kv(l, normed, OWN)
        project_q(l, normed)

    def prepare(l, pieces):
        project_kv(l, norm(l, stream_of(l, pieces)), pieces)

    def build_hidden():
        k = lax.broadcasted_iota(jnp.int32, (1, slab), 1)
        key_row = k // slab_cols
        key_col = k - key_row * slab_cols
        row0 = row_index * tile_rows
        col0 = col_index * tile_cols
        c = lax.broadcasted_iota(jnp.int32, (tile_cols, 1), 0)
        col_start = jnp.clip(col0 + c - HALF_COLS, 0, tp_count * tile_cols - WIN_COLS)
        col_start = col_start - (col0 - HALF_COLS)
        col_inside = (key_col >= col_start) & (key_col < col_start + WIN_COLS)
        for r in range(tile_rows):
            start = jnp.clip(row0 + r - HALF_ROWS, 0, sp_count * tile_rows - WIN_ROWS)
            start = start - (row0 - HALF_ROWS)
            row_inside = (key_row >= start) & (key_row < start + WIN_ROWS)
            hidden[r * tile_cols : (r + 1) * tile_cols] = jnp.where(
                col_inside & row_inside, 0.0, HIDDEN
            )

    lead = tile_rows - 1 - BELOW

    def build_flat():
        row_count, col_count = 2 * WIN_ROWS - 1, 2 * WIN_COLS - 1
        flat[...] = jnp.zeros_like(flat)
        for l in range(layers):
            for a in range(row_count):
                place = (lead + a) * slab_cols
                flat[l * heads : (l + 1) * heads, place : place + col_count] = bias[l, a] * LOG2E

    def build_table(l):
        width = flat.shape[1]
        shift = (width - (WIN_COLS - 1 - HALF_COLS)) % width
        for h in range(heads):
            row = l * heads + h
            spread = jnp.broadcast_to(flat[row : row + 1, :], (tile_cols, width))
            wide[...] = pltpu.roll(spread, shift, 1, stride=1, stride_axis=0)
            for r in range(HALF_ROWS):
                first_lane = (tile_rows - 1 - r) * slab_cols
                seen = wide[:, first_lane : first_lane + slab - edge]
                for low in (0, edge):
                    start = r * tile_cols + (half if low else 0)
                    rows = slice(start, start + tile_cols)
                    keys = slice(low, low + slab - edge)
                    table[l, h, rows, keys] = seen + hidden[rows, keys]

    def keys_values(rows):
        count = (rows.stop - rows.start) * slab_cols
        return kv[rows].astype(jnp.float32).reshape(count, 2 * inner).astype(jnp.bfloat16)

    def score(l, h, span, keys, lanes):
        return lax.dot_general(
            queries[span, h * HEAD_DIM : (h + 1) * HEAD_DIM], keys,
            (((1,), (1,)), ((), ())), preferred_element_type=jnp.float32,
        ) + table[l, h, span, lanes]

    def weigh(expo, values):
        ones = jnp.ones(values.shape, jnp.bfloat16)
        return jnp.dot(
            expo, jnp.concatenate([values, ones], axis=1),
            preferred_element_type=jnp.float32,
        )

    def attend_own(l):
        both = keys_values(own_rows)
        for h in range(heads):
            keys = both[:, h * HEAD_DIM : (h + 1) * HEAD_DIM]
            values = both[:, inner + h * HEAD_DIM : inner + (h + 1) * HEAD_DIM]
            scores = score(l, h, slice(0, tokens), keys, slice(edge, slab - edge))
            top = jnp.max(scores, axis=1, keepdims=True)
            tops[h] = jnp.broadcast_to(top, (tokens, HEAD_DIM))
            mixes[h] = weigh(jnp.exp2(scores - top).astype(jnp.bfloat16), values)

    def attend_edges(l):
        both = jnp.concatenate([keys_values(rows) for rows, _ in EDGES])
        none = jnp.zeros((half, edge), jnp.bfloat16)
        mixture = []
        for h in range(heads):
            column = slice(h * HEAD_DIM, (h + 1) * HEAD_DIM)
            scores = lax.dot_general(
                queries[:, column], both[:, column],
                (((1,), (1,)), ((), ())), preferred_element_type=jnp.float32,
            )
            scores = jnp.concatenate([
                scores[:half, :edge] + table[l, h, :half, :edge],
                scores[half:, edge:] + table[l, h, half:, slab - edge :],
            ])
            top = jnp.maximum(tops[h], jnp.max(scores, axis=1, keepdims=True))
            scale = jnp.exp2(tops[h] - top)
            expo = jnp.exp2(scores - top).astype(jnp.bfloat16)
            expo = jnp.concatenate([
                jnp.concatenate([expo[:half], none], axis=1),
                jnp.concatenate([none, expo[half:]], axis=1),
            ])
            found = weigh(expo, both[:, inner + h * HEAD_DIM : inner + (h + 1) * HEAD_DIM])
            mix = mixes[h, :, :HEAD_DIM] * scale + found[:, :HEAD_DIM]
            total = mixes[h, :, HEAD_DIM:] * scale + found[:, HEAD_DIM:]
            mixture.append((mix / total).astype(jnp.bfloat16))
        return jnp.concatenate(mixture, axis=1)

    def finish(l, mixture):
        stream = acc[...] + jnp.dot(mixture, wo[l], preferred_element_type=jnp.float32)
        return stream.astype(jnp.bfloat16)

    zero_missing()
    first[0].wait()
    count = sum(jnp.where(exists, 1, 0).astype(jnp.int32) for _, _, exists in neighbours)
    pl.semaphore_wait(barrier, count)
    OUTGOING = [
        "D_inner", "U_inner", "C_far", "D_outer", "U_outer", "D_diag", "U_diag", "C_beside",
    ]
    send(0, OUTGOING)
    fetch(0, "o")
    for later in range(1, layers):
        fetch(later, "kvqo")
    first[1].wait()
    acc[...] = gather(xs, OWN)
    for l in range(layers):
        prepare_own(l)
        if l == 0:
            build_hidden()
            first[2].wait()
            build_flat()
        build_table(l)
        pass_on(l, "U")
        pass_on(l, "D")
        receive(l, ["C_beside", "C_far"])
        if l == 0:
            arrived(l, "o")
        prepare(l, SIDES)
        attend_own(l)
        receive(l, [way + what for way in "UD" for what in ("_outer", "_diag", "_relay")])
        prepare(l, EDGES)
        mixture = attend_edges(l)
        if l < layers - 1:
            ms[l, own_rows, own_cols] = (
                mixture.astype(jnp.float32)
                .reshape(tile_rows, own_blocks, HALF_COLS, inner)
                .astype(jnp.bfloat16)
            )
            send(l + 1, OUTGOING)
            acc[...] = finish(l, mixture).astype(jnp.float32)
        else:
            arrived(l, "o")
            out[...] = finish(l, mixture).reshape(out.shape)
    for l in range(layers):
        for kind in KINDS:
            @pl.when(plan(kind)[6])
            def _():
                halo_copy(l, kind).wait_send()


def on_device(sp_count, tp_count, grid_tokens, norm_gain, w_query, w_key, w_value, offset_bias, w_out):
    tile_rows, tile_cols, model_width = grid_tokens.shape
    layers, _, inner = w_query.shape
    tokens = tile_rows * tile_cols
    heads = inner // HEAD_DIM
    slab_rows = tile_rows + WIN_ROWS
    slab_cols = tile_cols + WIN_COLS
    slab = slab_rows * slab_cols
    flat_width = -(-(slab + tile_rows * slab_cols) // 128) * 128
    blocks = slab_cols // HALF_COLS
    bias_rows = jnp.transpose(offset_bias, (0, 2, 1, 3))
    blocked = grid_tokens.reshape(tile_rows, tile_cols // HALF_COLS, HALF_COLS, model_width)
    bf16, f32 = jnp.bfloat16, jnp.float32
    hbm = pl.BlockSpec(memory_space=pltpu.HBM)
    return pl.pallas_call(
        functools.partial(kernel, sp_count=sp_count, tp_count=tp_count),
        out_shape=jax.ShapeDtypeStruct(grid_tokens.shape, bf16),
        in_specs=[hbm] * 7,
        out_specs=pl.BlockSpec(memory_space=pltpu.VMEM),
        scratch_shapes=[
            pltpu.VMEM((slab_rows, blocks, HALF_COLS, model_width), bf16),
            pltpu.VMEM((max(layers - 1, 1), slab_rows, blocks, HALF_COLS, inner), bf16),
            pltpu.VMEM(norm_gain.shape, f32),
            pltpu.VMEM(w_query.shape, bf16),
            pltpu.VMEM(w_key.shape, bf16),
            pltpu.VMEM(w_value.shape, bf16),
            pltpu.VMEM(w_out.shape, bf16),
            pltpu.VMEM(bias_rows.shape, f32),
            pltpu.VMEM((layers * heads, flat_width), f32),
            pltpu.VMEM((tile_cols, flat_width), f32),
            pltpu.VMEM((tokens, slab), f32),
            pltpu.VMEM((layers, heads, tokens, slab), f32),
            pltpu.VMEM((slab_rows, blocks, HALF_COLS, 2 * inner), bf16),
            pltpu.VMEM((tokens, inner), bf16),
            pltpu.VMEM((tokens, model_width), f32),
            pltpu.VMEM((heads, tokens, HEAD_DIM), f32),
            pltpu.VMEM((heads, tokens, 2 * HEAD_DIM), f32),
            pltpu.SemaphoreType.DMA((3,)),
            pltpu.SemaphoreType.DMA((layers, 4)),
            pltpu.SemaphoreType.DMA((layers, len(KINDS))),
            pltpu.SemaphoreType.DMA((layers, len(KINDS))),
        ],
        compiler_params=pltpu.CompilerParams(
            collective_id=0, has_side_effects=True, vmem_limit_bytes=54784 * 1024
        ),
    )(
        blocked, pltpu.with_memory_space_constraint(norm_gain, pltpu.HBM), w_query, w_key,
        w_value, pltpu.with_memory_space_constraint(bias_rows, pltpu.HBM), w_out,
    )


def solution(mesh):
    return jax.shard_map(
        functools.partial(on_device, mesh.shape["sp"], mesh.shape["tp"]),
        mesh=mesh,
        in_specs=(P(("grp", "sp"), "tp", None), P(), P(), P(), P(), P(), P()),
        out_specs=P(("grp", "sp"), "tp", None),
        check_vma=False,
    )
```

time: 19.7 us -> 17.8 us (0.904)
  Pallas kernels: 18.7 us -> 16.9 us
    pallas_call x1, Pallas kernels: 18.7 us -> 16.9 us  [on_device(): pl.pallas_call(functools.partial(kernel, sp_count=sp_count, tp_count=tp_c...]
where the time goes in v2:
time: 17.8 us; the launch traced here: 17.6 us
  Pallas kernels  16.9 us (95%)
  local copies, waits for them, and re-layouts  0.71 us (4%)
    pallas_call x1, Pallas kernels, on_device(): pl.pallas_call(functools.partial(kernel, sp_count=sp_count, tp_count=tp_c...  16.9 us
    unnamed x1, local copies, waits for them, and re-layouts  0.71 us

profile of v2, /device:TPU:1, one launch (start us, length us, event | category | flops | bytes accessed | tf_op | source)
XLA Modules:
  0.0 17.6 jit_solution(14808338267818977530)
XLA Ops:
  0.0 16.9 %shard_map.73 = bf16[8,16,1024]{2,1,0:T(8,128)(2,1)S(1)} custom-call(bf16[8,2,8,1024]{3,2,1,0:T(8,128)(2,1)} %bitcast.2, f32[2,1024]{1,0:T(2,128)} %gain_hbm.1, bf16[2,1024,512]{2,1,0:T(8,128)(2,1)} %wq_hbm.1, bf16[2,1024,512]{2,1,0:T(8,128)(2,1)} %wk_hbm.1, bf16[2,1024,512]{2,1,0:T(8,128)(2,1)} %wv_hbm.1, f32[2,15,4,31]{3,2,1,0:T(4,128)} %bitcast.3, ...), custom_call_target="tpu_custom_call" | custom-call | tf_op jit(solution)/shard_map/pallas_call | solution.py:387
  16.9 0.7 %copy.9 = bf16[8,16,1024]{2,1,0:T(8,128)(2,1)} copy(bf16[8,16,1024]{2,1,0:T(8,128)(2,1)S(1)} %shard_map.73) | data formatting | bytes 524288

commit v3 on v2

--- a/solution.py
+++ b/solution.py
@@ -65,9 +65,9 @@
     below_rows = slice(HALF_ROWS + tile_rows, HALF_ROWS + tile_rows + BELOW)
     OWN = ((own_rows, own_cols),)
     SIDES = ((own_rows, slice(0, 1)), (own_rows, slice(own_blocks + 1, own_blocks + 2)))
-    EDGES = (
-        (above_rows, every_block), (slice(slab_rows - HALF_ROWS, slab_rows), every_block),
-    )
+    ABOVE = (above_rows, every_block)
+    BENEATH = (slice(slab_rows - HALF_ROWS, slab_rows), every_block)
+    EDGES = ABOVE, BENEATH
 
     barrier = pltpu.get_barrier_semaphore()
     for dr, dc, exists in neighbours:
@@ -97,9 +97,9 @@
             copy.start()
             weight_copies[l, name] = copy
 
-    def arrived(l, name):
-        if (l, name) in weight_copies:
-            weight_copies.pop((l, name)).wait()
+    def arrived(l, names):
+        for name in names:
+            weight_copies[l, name].wait()
 
     fetch(0, "kvq")
 
@@ -129,7 +129,7 @@
         return pltpu.make_async_remote_copy(
             src_ref=ref.at[src_rows, pl.ds(src_block, 1)],
             dst_ref=ref.at[dst_rows, pl.ds(dst_block, 1)],
-            send_sem=send_sem.at[l, i],
+            send_sem=send_sem.at[i],
             recv_sem=recv_sem.at[l, i],
             device_id={"sp": row_index + dr, "tp": col_index + dc},
             device_id_type=MESH,
@@ -147,34 +147,34 @@
             def _():
                 halo_copy(l, kind).wait_recv()
 
+    def sent(l):
+        for kind in KINDS:
+            @pl.when(plan(kind)[6])
+            def _():
+                halo_copy(l, kind).wait_send()
+
     def pass_on(l, way):
         receive(l, [way + "_inner"])
         send(l, [way + "_relay"])
 
-    def fill(rows, cols):
-        for ref in [xs] + [ms.at[l] for l in range(layers - 1)]:
-            shape = (rows.stop - rows.start, cols.stop - cols.start) + ref.shape[2:]
-            ref[rows, cols] = jnp.zeros(shape, jnp.bfloat16)
+    def zero(ref, rows, cols):
+        shape = (rows.stop - rows.start, cols.stop - cols.start) + ref.shape[2:]
+        ref[rows, cols] = jnp.zeros(shape, jnp.bfloat16)
 
     def zero_missing():
-        received = slice(0, slab_rows - 1)
-        fill(slice(slab_rows - 1, slab_rows), every_block)
-
-        @pl.when(jnp.logical_not(has_above))
-        def _():
-            fill(above_rows, every_block)
-
-        @pl.when(jnp.logical_not(has_below))
-        def _():
-            fill(below_rows, every_block)
-
-        @pl.when(col_index == 0)
-        def _():
-            fill(received, slice(0, 1))
-
-        @pl.when(col_index == tp_count - 1)
-        def _():
-            fill(received, slice(own_blocks + 1, own_blocks + 2))
+        exchanged = [xs] + [ms.at[l] for l in range(layers - 1)]
+        for ref in exchanged:
+            zero(ref, slice(slab_rows - 1, slab_rows), every_block)
+        for exists, piece in ((has_above, ABOVE), (has_below, BENEATH)):
+            @pl.when(jnp.logical_not(exists))
+            def _():
+                zero(kv, *piece)
+
+        for block in (0, own_blocks + 1):
+            @pl.when(col_index == (0 if block == 0 else tp_count - 1))
+            def _():
+                for ref in exchanged:
+                    zero(ref, slice(0, slab_rows - 1), slice(block, block + 1))
 
     def gather(ref, pieces):
         width = ref.shape[-1]
@@ -195,8 +195,7 @@
         return stream
 
     def project_kv(l, normed, pieces):
-        for i, (name, w) in enumerate((("k", wk), ("v", wv))):
-            arrived(l, name)
+        for i, w in enumerate((wk, wv)):
             made = jnp.dot(normed, w[l], preferred_element_type=jnp.float32)
             place = 0
             for rows, cols in pieces:
@@ -208,7 +207,6 @@
                 place += count
 
     def project_q(l, normed):
-        arrived(l, "q")
         made = jnp.dot(normed, wq[l], preferred_element_type=jnp.float32)
         queries[...] = (made * (LOG2E / HEAD_DIM**0.5)).astype(jnp.bfloat16)
 
@@ -251,18 +249,21 @@
     def build_table(l):
         width = flat.shape[1]
         shift = (width - (WIN_COLS - 1 - HALF_COLS)) % width
-        for h in range(heads):
-            row = l * heads + h
-            spread = jnp.broadcast_to(flat[row : row + 1, :], (tile_cols, width))
-            wide[...] = pltpu.roll(spread, shift, 1, stride=1, stride_axis=0)
+
+        def one_head(h, carry):
+            spread = jnp.broadcast_to(flat[pl.ds(l * heads + h, 1), :], (tile_cols, width))
+            turned = pltpu.roll(spread, shift, 1, stride=1, stride_axis=0)
             for r in range(HALF_ROWS):
                 first_lane = (tile_rows - 1 - r) * slab_cols
-                seen = wide[:, first_lane : first_lane + slab - edge]
+                seen = turned[:, first_lane : first_lane + slab - edge]
                 for low in (0, edge):
                     start = r * tile_cols + (half if low else 0)
                     rows = slice(start, start + tile_cols)
                     keys = slice(low, low + slab - edge)
                     table[l, h, rows, keys] = seen + hidden[rows, keys]
+            return carry
+
+        lax.fori_loop(0, heads, one_head, 0)
 
     def keys_values(rows):
         count = (rows.stop - rows.start) * slab_cols
@@ -319,38 +320,59 @@
         return jnp.concatenate(mixture, axis=1)
 
     def finish(l, mixture):
-        stream = acc[...] + jnp.dot(mixture, wo[l], preferred_element_type=jnp.float32)
-        return stream.astype(jnp.bfloat16)
+        for low in range(0, model_width, 2 * HEAD_DIM):
+            cols = slice(low, low + 2 * HEAD_DIM)
+            stream = acc[:, cols] + jnp.dot(
+                mixture, wo[l, :, cols], preferred_element_type=jnp.float32
+            )
+            stream = stream.astype(jnp.bfloat16)
+            if l == layers - 1:
+                out[:, :, cols] = stream.reshape(tile_rows, tile_cols, 2 * HEAD_DIM)
+            else:
+                acc[:, cols] = stream.astype(jnp.float32)
 
     zero_missing()
     first[0].wait()
     count = sum(jnp.where(exists, 1, 0).astype(jnp.int32) for _, _, exists in neighbours)
     pl.semaphore_wait(barrier, count)
-    OUTGOING = [
-        "D_inner", "U_inner", "C_far", "D_outer", "U_outer", "D_diag", "U_diag", "C_beside",
-    ]
-    send(0, OUTGOING)
+    EARLY = ["C_beside", "D_inner", "U_inner", "C_far"]
+    LATE = ["D_outer", "U_outer", "D_diag", "U_diag"]
+    send(0, EARLY)
     fetch(0, "o")
     for later in range(1, layers):
         fetch(later, "kvqo")
     first[1].wait()
     acc[...] = gather(xs, OWN)
     for l in range(layers):
+        if l == 0:
+            arrived(0, "kvq")
         prepare_own(l)
         if l == 0:
+            send(0, LATE)
             build_hidden()
             first[2].wait()
             build_flat()
         build_table(l)
+        if l == 0:
+            arrived(0, "o")
+            for later in range(1, layers):
+                arrived(later, "kvqo")
         pass_on(l, "U")
         pass_on(l, "D")
         receive(l, ["C_beside", "C_far"])
-        if l == 0:
-            arrived(l, "o")
         prepare(l, SIDES)
         attend_own(l)
         receive(l, [way + what for way in "UD" for what in ("_outer", "_diag", "_relay")])
-        prepare(l, EDGES)
+        if l == layers - 1:
+            sent(l)
+        for exist, pieces in (
+            (has_above & has_below, EDGES),
+            (has_above & jnp.logical_not(has_below), EDGES[:1]),
+            (jnp.logical_not(has_above) & has_below, EDGES[1:]),
+        ):
+            @pl.when(exist)
+            def _():
+                prepare(l, pieces)
         mixture = attend_edges(l)
         if l < layers - 1:
             ms[l, own_rows, own_cols] = (
@@ -358,16 +380,12 @@
                 .reshape(tile_rows, own_blocks, HALF_COLS, inner)
                 .astype(jnp.bfloat16)
             )
-            send(l + 1, OUTGOING)
-            acc[...] = finish(l, mixture).astype(jnp.float32)
+            sent(l)
+            send(l + 1, EARLY)
+            finish(l, mixture)
+            send(l + 1, LATE)
         else:
-            arrived(l, "o")
-            out[...] = finish(l, mixture).reshape(out.shape)
-    for l in range(layers):
-        for kind in KINDS:
-            @pl.when(plan(kind)[6])
-            def _():
-                halo_copy(l, kind).wait_send()
+            finish(l, mixture)
 
 
 def on_device(sp_count, tp_count, grid_tokens, norm_gain, w_query, w_key, w_value, offset_bias, w_out):
@@ -409,7 +427,7 @@
             pltpu.VMEM((heads, tokens, 2 * HEAD_DIM), f32),
             pltpu.SemaphoreType.DMA((3,)),
             pltpu.SemaphoreType.DMA((layers, 4)),
-            pltpu.SemaphoreType.DMA((layers, len(KINDS))),
+            pltpu.SemaphoreType.DMA((len(KINDS),)),
             pltpu.SemaphoreType.DMA((layers, len(KINDS))),
         ],
         compiler_params=pltpu.CompilerParams(

time: 17.8 us -> 17.4 us (0.978)
  Pallas kernels: 16.9 us -> 16.6 us
    pallas_call x1, Pallas kernels: 16.9 us -> 16.6 us  [on_device(): pl.pallas_call(functools.partial(kernel, sp_count=sp_count, tp_count=tp_c...]
where the time goes in v3:
time: 17.4 us; the launch traced here: 17.3 us
  Pallas kernels  16.6 us (95%)
  local copies, waits for them, and re-layouts  0.71 us (4%)
    pallas_call x1, Pallas kernels, on_device(): pl.pallas_call(functools.partial(kernel, sp_count=sp_count, tp_count=tp_c...  16.6 us
    unnamed x1, local copies, waits for them, and re-layouts  0.71 us

profile of v3, /device:TPU:1, one launch (start us, length us, event | category | flops | bytes accessed | tf_op | source)
XLA Modules:
  0.0 17.3 jit_solution(11005151012669343506)
XLA Ops:
  0.0 16.6 %shard_map.73 = bf16[8,16,1024]{2,1,0:T(8,128)(2,1)S(1)} custom-call(bf16[8,2,8,1024]{3,2,1,0:T(8,128)(2,1)} %bitcast.2, f32[2,1024]{1,0:T(2,128)} %gain_hbm.1, bf16[2,1024,512]{2,1,0:T(8,128)(2,1)} %wq_hbm.1, bf16[2,1024,512]{2,1,0:T(8,128)(2,1)} %wk_hbm.1, bf16[2,1024,512]{2,1,0:T(8,128)(2,1)} %wv_hbm.1, f32[2,15,4,31]{3,2,1,0:T(4,128)} %bitcast.3, ...), custom_call_target="tpu_custom_call" | custom-call | tf_op jit(solution)/shard_map/pallas_call | solution.py:405
  16.6 0.7 %copy.9 = bf16[8,16,1024]{2,1,0:T(8,128)(2,1)} copy(bf16[8,16,1024]{2,1,0:T(8,128)(2,1)S(1)} %shard_map.73) | data formatting | bytes 524288

commit v4 on v3

--- a/solution.py
+++ b/solution.py
@@ -28,7 +28,7 @@
 def kernel(
     x_hbm, gain_hbm, wq_hbm, wk_hbm, wv_hbm, bias_hbm, wo_hbm, out,
     xs, ms, gain, wq, wk, wv, wo, bias, flat, wide, hidden, table, kv, queries, acc, tops, mixes,
-    local_sem, w_sem, send_sem, recv_sem,
+    local_sem, w_sem, send_sem, recv_sem, entered_sem,
     *, sp_count, tp_count,
 ):
     layers, model_width, inner = wq.shape
@@ -52,8 +52,7 @@
     has_beside = (col_index + beside >= 0) & (col_index + beside < tp_count)
     has_far = (col_index + far >= 0) & (col_index + far < tp_count)
     neighbours = (
-        (-1, 0, has_above), (1, 0, has_below), (-1, far, has_above & has_far),
-        (1, far, has_below & has_far), (0, far, has_far), (0, beside, has_beside),
+        (-1, 0, has_above), (1, 0, has_below), (0, far, has_far), (0, beside, has_beside),
     )
 
     own_rows = slice(HALF_ROWS, HALF_ROWS + tile_rows)
@@ -64,9 +63,10 @@
     first_rows = slice(HALF_ROWS, HALF_ROWS + BELOW)
     below_rows = slice(HALF_ROWS + tile_rows, HALF_ROWS + tile_rows + BELOW)
     OWN = ((own_rows, own_cols),)
-    SIDES = ((own_rows, slice(0, 1)), (own_rows, slice(own_blocks + 1, own_blocks + 2)))
+    BESIDE = (own_rows, pl.ds(right_block, 1))
+    FAR = (own_rows, pl.ds(left_block, 1))
     ABOVE = (above_rows, every_block)
-    BENEATH = (slice(slab_rows - HALF_ROWS, slab_rows), every_block)
+    BENEATH = (below_rows, every_block)
     EDGES = ABOVE, BENEATH
 
     barrier = pltpu.get_barrier_semaphore()
@@ -157,18 +157,25 @@
         receive(l, [way + "_inner"])
         send(l, [way + "_relay"])
 
+    def shape_of(rows, cols):
+        blocks = cols.size if isinstance(cols, pl.Slice) else cols.stop - cols.start
+        return rows.stop - rows.start, blocks, HALF_COLS
+
     def zero(ref, rows, cols):
-        shape = (rows.stop - rows.start, cols.stop - cols.start) + ref.shape[2:]
+        shape = shape_of(rows, cols) + ref.shape[3:]
         ref[rows, cols] = jnp.zeros(shape, jnp.bfloat16)
 
     def zero_missing():
         exchanged = [xs] + [ms.at[l] for l in range(layers - 1)]
-        for ref in exchanged:
-            zero(ref, slice(slab_rows - 1, slab_rows), every_block)
+        zero(kv, slice(slab_rows - 1, slab_rows), every_block)
         for exists, piece in ((has_above, ABOVE), (has_below, BENEATH)):
             @pl.when(jnp.logical_not(exists))
             def _():
                 zero(kv, *piece)
+
+        @pl.when(jnp.logical_not(has_far))
+        def _():
+            zero(kv, *FAR)
 
         for block in (0, own_blocks + 1):
             @pl.when(col_index == (0 if block == 0 else tp_count - 1))
@@ -199,7 +206,7 @@
             made = jnp.dot(normed, w[l], preferred_element_type=jnp.float32)
             place = 0
             for rows, cols in pieces:
-                shape = (rows.stop - rows.start, cols.stop - cols.start, HALF_COLS)
+                shape = shape_of(rows, cols)
                 count = math.prod(shape)
                 kv[rows, cols, :, i * inner : (i + 1) * inner] = (
                     made[place : place + count].reshape(*shape, inner).astype(jnp.bfloat16)
@@ -293,7 +300,8 @@
             mixes[h] = weigh(jnp.exp2(scores - top).astype(jnp.bfloat16), values)
 
     def attend_edges(l):
-        both = jnp.concatenate([keys_values(rows) for rows, _ in EDGES])
+        beyond = above_rows, slice(slab_rows - HALF_ROWS, slab_rows)
+        both = jnp.concatenate([keys_values(rows) for rows in beyond])
         none = jnp.zeros((half, edge), jnp.bfloat16)
         mixture = []
         for h in range(heads):
@@ -336,8 +344,17 @@
     count = sum(jnp.where(exists, 1, 0).astype(jnp.int32) for _, _, exists in neighbours)
     pl.semaphore_wait(barrier, count)
     EARLY = ["C_beside", "D_inner", "U_inner", "C_far"]
-    LATE = ["D_outer", "U_outer", "D_diag", "U_diag"]
+    OUTER, DIAG = ["D_outer", "U_outer"], ["D_diag", "U_diag"]
     send(0, EARLY)
+    for way, (dr, exists) in enumerate(((-1, has_above), (1, has_below))):
+        @pl.when(exists & has_far)
+        def _():
+            pl.semaphore_signal(
+                entered_sem.at[way],
+                inc=1,
+                device_id={"sp": row_index + dr, "tp": col_index},
+                device_id_type=MESH,
+            )
     fetch(0, "o")
     for later in range(1, layers):
         fetch(later, "kvqo")
@@ -346,9 +363,15 @@
     for l in range(layers):
         if l == 0:
             arrived(0, "kvq")
+            send(0, OUTER)
         prepare_own(l)
         if l == 0:
-            send(0, LATE)
+            for way, exists in enumerate((has_below, has_above)):
+                @pl.when(exists & has_far)
+                def _():
+                    pl.semaphore_wait(entered_sem.at[way], 1)
+
+            send(0, DIAG)
             build_hidden()
             first[2].wait()
             build_flat()
@@ -357,22 +380,44 @@
             arrived(0, "o")
             for later in range(1, layers):
                 arrived(later, "kvqo")
+        receive(l, ["C_beside"])
+        prepare(l, (BESIDE,))
+
+        @pl.when(jnp.logical_not(has_far))
+        def _():
+            attend_own(l)
+
         pass_on(l, "U")
         pass_on(l, "D")
-        receive(l, ["C_beside", "C_far"])
-        prepare(l, SIDES)
-        attend_own(l)
-        receive(l, [way + what for way in "UD" for what in ("_outer", "_diag", "_relay")])
+        receive(l, ["C_far"])
+
+        @pl.when(has_far)
+        def _():
+            prepare(l, (FAR,))
+            attend_own(l)
+
+        arrivals = {
+            way: [way + "_" + what for what in ("outer", "diag", "relay")] for way in "UD"
+        }
+        if l == 0:
+            for way, exists, piece in (("U", has_below, BENEATH), ("D", has_above, ABOVE)):
+                receive(l, arrivals[way])
+
+                @pl.when(exists)
+                def _():
+                    prepare(l, (piece,))
+        else:
+            receive(l, arrivals["U"] + arrivals["D"])
+            for exist, pieces in (
+                (has_above & has_below, EDGES),
+                (has_above & jnp.logical_not(has_below), EDGES[:1]),
+                (jnp.logical_not(has_above) & has_below, EDGES[1:]),
+            ):
+                @pl.when(exist)
+                def _():
+                    prepare(l, pieces)
         if l == layers - 1:
             sent(l)
-        for exist, pieces in (
-            (has_above & has_below, EDGES),
-            (has_above & jnp.logical_not(has_below), EDGES[:1]),
-            (jnp.logical_not(has_above) & has_below, EDGES[1:]),
-        ):
-            @pl.when(exist)
-            def _():
-                prepare(l, pieces)
         mixture = attend_edges(l)
         if l < layers - 1:
             ms[l, own_rows, own_cols] = (
@@ -383,7 +428,7 @@
             sent(l)
             send(l + 1, EARLY)
             finish(l, mixture)
-            send(l + 1, LATE)
+            send(l + 1, OUTER + DIAG)
         else:
             finish(l, mixture)
 
@@ -429,6 +474,7 @@
             pltpu.SemaphoreType.DMA((layers, 4)),
             pltpu.SemaphoreType.DMA((len(KINDS),)),
             pltpu.SemaphoreType.DMA((layers, len(KINDS))),
+            pltpu.SemaphoreType.REGULAR((2,)),
         ],
         compiler_params=pltpu.CompilerParams(
             collective_id=0, has_side_effects=True, vmem_limit_bytes=54784 * 1024

time: 17.4 us -> 17.2 us (0.989)
  the two profiles are of different devices: /device:TPU:1 before, /device:TPU:17 now
where the time goes in v4:
time: 17.2 us; the launch traced here: 17.1 us
  Pallas kernels  16.4 us (95%)
  local copies, waits for them, and re-layouts  0.71 us (4%)
    pallas_call x1, Pallas kernels, on_device(): pl.pallas_call(functools.partial(kernel, sp_count=sp_count, tp_count=tp_c...  16.4 us
    unnamed x1, local copies, waits for them, and re-layouts  0.71 us

profile of v4, /device:TPU:17, one launch (start us, length us, event | category | flops | bytes accessed | tf_op | source)
XLA Modules:
  0.0 17.1 jit_solution(9224190038179160989)
XLA Ops:
  0.0 16.4 %shard_map.73 = bf16[8,16,1024]{2,1,0:T(8,128)(2,1)S(1)} custom-call(bf16[8,2,8,1024]{3,2,1,0:T(8,128)(2,1)} %bitcast.2, f32[2,1024]{1,0:T(2,128)} %gain_hbm.1, bf16[2,1024,512]{2,1,0:T(8,128)(2,1)} %wq_hbm.1, bf16[2,1024,512]{2,1,0:T(8,128)(2,1)} %wk_hbm.1, bf16[2,1024,512]{2,1,0:T(8,128)(2,1)} %wv_hbm.1, f32[2,15,4,31]{3,2,1,0:T(4,128)} %bitcast.3, ...), custom_call_target="tpu_custom_call" | custom-call | tf_op jit(solution)/shard_map/pallas_call | solution.py:450
  16.4 0.7 %copy.9 = bf16[8,16,1024]{2,1,0:T(8,128)(2,1)} copy(bf16[8,16,1024]{2,1,0:T(8,128)(2,1)S(1)} %shard_map.73) | data formatting | bytes 524288

commit v5 on v4

--- a/solution.py
+++ b/solution.py
@@ -191,7 +191,7 @@
 
     def norm(l, stream):
         factor = lax.rsqrt(jnp.mean(stream * stream, axis=-1, keepdims=True) + NORM_EPSILON)
-        return (stream * factor * gain[l : l + 1]).astype(jnp.bfloat16)
+        return (stream * gain[l : l + 1]).astype(jnp.bfloat16), factor
 
     def stream_of(l, pieces):
         stream = gather(xs, pieces)
@@ -202,8 +202,9 @@
         return stream
 
     def project_kv(l, normed, pieces):
+        scaled, factor = normed
         for i, w in enumerate((wk, wv)):
-            made = jnp.dot(normed, w[l], preferred_element_type=jnp.float32)
+            made = jnp.dot(scaled, w[l], preferred_element_type=jnp.float32) * factor
             place = 0
             for rows, cols in pieces:
                 shape = shape_of(rows, cols)
@@ -214,8 +215,9 @@
                 place += count
 
     def project_q(l, normed):
-        made = jnp.dot(normed, wq[l], preferred_element_type=jnp.float32)
-        queries[...] = (made * (LOG2E / HEAD_DIM**0.5)).astype(jnp.bfloat16)
+        scaled, factor = normed
+        made = jnp.dot(scaled, wq[l], preferred_element_type=jnp.float32)
+        queries[...] = (made * (factor * (LOG2E / HEAD_DIM**0.5))).astype(jnp.bfloat16)
 
     def prepare_own(l):
         normed = norm(l, acc[...])
@@ -400,7 +402,7 @@
             way: [way + "_" + what for what in ("outer", "diag", "relay")] for way in "UD"
         }
         if l == 0:
-            for way, exists, piece in (("U", has_below, BENEATH), ("D", has_above, ABOVE)):
+            for way, exists, piece in (("D", has_above, ABOVE), ("U", has_below, BENEATH)):
                 receive(l, arrivals[way])
 
                 @pl.when(exists)

time: 17.2 us -> 16.4 us (0.953)
  the two profiles are of different devices: /device:TPU:17 before, /device:TPU:1 now
where the time goes in v5:
time: 16.4 us; the launch traced here: 16.2 us
  Pallas kernels  15.5 us (95%)
  local copies, waits for them, and re-layouts  0.71 us (4%)
    pallas_call x1, Pallas kernels, on_device(): pl.pallas_call(functools.partial(kernel, sp_count=sp_count, tp_count=tp_c...  15.5 us
    unnamed x1, local copies, waits for them, and re-layouts  0.71 us

profile of v5, /device:TPU:1, one launch (start us, length us, event | category | flops | bytes accessed | tf_op | source)
XLA Modules:
  0.0 16.2 jit_solution(5288755497296628689)
XLA Ops:
  0.0 15.5 %shard_map.73 = bf16[8,16,1024]{2,1,0:T(8,128)(2,1)S(1)} custom-call(bf16[8,2,8,1024]{3,2,1,0:T(8,128)(2,1)} %bitcast.2, f32[2,1024]{1,0:T(2,128)} %gain_hbm.1, bf16[2,1024,512]{2,1,0:T(8,128)(2,1)} %wq_hbm.1, bf16[2,1024,512]{2,1,0:T(8,128)(2,1)} %wk_hbm.1, bf16[2,1024,512]{2,1,0:T(8,128)(2,1)} %wv_hbm.1, f32[2,15,4,31]{3,2,1,0:T(4,128)} %bitcast.3, ...), custom_call_target="tpu_custom_call" | custom-call | tf_op jit(solution)/shard_map/pallas_call | solution.py:452
  15.5 0.7 %copy.9 = bf16[8,16,1024]{2,1,0:T(8,128)(2,1)} copy(bf16[8,16,1024]{2,1,0:T(8,128)(2,1)S(1)} %shard_map.73) | data formatting | bytes 524288

commit v6 on v5

--- a/solution.py
+++ b/solution.py
@@ -27,7 +27,7 @@
 
 def kernel(
     x_hbm, gain_hbm, wq_hbm, wk_hbm, wv_hbm, bias_hbm, wo_hbm, out,
-    xs, ms, gain, wq, wk, wv, wo, bias, flat, wide, hidden, table, kv, queries, acc, tops, mixes,
+    xs, ms, gain, wq, wk, wv, wo, bias, flat, wide, hidden, table, kv, kv_edges, queries, acc, tops, mixes,
     local_sem, w_sem, send_sem, recv_sem, entered_sem,
     *, sp_count, tp_count,
 ):
@@ -167,11 +167,16 @@
 
     def zero_missing():
         exchanged = [xs] + [ms.at[l] for l in range(layers - 1)]
-        zero(kv, slice(slab_rows - 1, slab_rows), every_block)
-        for exists, piece in ((has_above, ABOVE), (has_below, BENEATH)):
+        beyond = edge + BELOW * slab_cols
+
+        def zero_edges(low, high):
+            kv_edges[low:high] = jnp.zeros((high - low, 2 * inner), jnp.bfloat16)
+
+        zero_edges(beyond, 2 * edge)
+        for exists, low, high in ((has_above, 0, edge), (has_below, edge, beyond)):
             @pl.when(jnp.logical_not(exists))
             def _():
-                zero(kv, *piece)
+                zero_edges(low, high)
 
         @pl.when(jnp.logical_not(has_far))
         def _():
@@ -209,9 +214,13 @@
             for rows, cols in pieces:
                 shape = shape_of(rows, cols)
                 count = math.prod(shape)
-                kv[rows, cols, :, i * inner : (i + 1) * inner] = (
-                    made[place : place + count].reshape(*shape, inner).astype(jnp.bfloat16)
-                )
+                values = made[place : place + count]
+                column = slice(i * inner, (i + 1) * inner)
+                if rows == own_rows:
+                    kv[rows, cols, :, column] = values.reshape(*shape, inner).astype(jnp.bfloat16)
+                else:
+                    low = 0 if rows == above_rows else edge
+                    kv_edges[low : low + count, column] = values.astype(jnp.bfloat16)
                 place += count
 
     def project_q(l, normed):
@@ -302,8 +311,7 @@
             mixes[h] = weigh(jnp.exp2(scores - top).astype(jnp.bfloat16), values)
 
     def attend_edges(l):
-        beyond = above_rows, slice(slab_rows - HALF_ROWS, slab_rows)
-        both = jnp.concatenate([keys_values(rows) for rows in beyond])
+        both = kv_edges[...]
         none = jnp.zeros((half, edge), jnp.bfloat16)
         mixture = []
         for h in range(heads):
@@ -389,8 +397,8 @@
         def _():
             attend_own(l)
 
+        pass_on(l, "D")
         pass_on(l, "U")
-        pass_on(l, "D")
         receive(l, ["C_far"])
 
         @pl.when(has_far)
@@ -401,23 +409,15 @@
         arrivals = {
             way: [way + "_" + what for what in ("outer", "diag", "relay")] for way in "UD"
         }
-        if l == 0:
-            for way, exists, piece in (("D", has_above, ABOVE), ("U", has_below, BENEATH)):
-                receive(l, arrivals[way])
-
-                @pl.when(exists)
-                def _():
-                    prepare(l, (piece,))
-        else:
-            receive(l, arrivals["U"] + arrivals["D"])
-            for exist, pieces in (
-                (has_above & has_below, EDGES),
-                (has_above & jnp.logical_not(has_below), EDGES[:1]),
-                (jnp.logical_not(has_above) & has_below, EDGES[1:]),
-            ):
-                @pl.when(exist)
-                def _():
-                    prepare(l, pieces)
+        receive(l, arrivals["U"] + arrivals["D"])
+        for exist, pieces in (
+            (has_above & has_below, EDGES),
+            (has_above & jnp.logical_not(has_below), EDGES[:1]),
+            (jnp.logical_not(has_above) & has_below, EDGES[1:]),
+        ):
+            @pl.when(exist)
+            def _():
+                prepare(l, pieces)
         if l == layers - 1:
             sent(l)
         mixture = attend_edges(l)
@@ -468,6 +468,7 @@
             pltpu.VMEM((tokens, slab), f32),
             pltpu.VMEM((layers, heads, tokens, slab), f32),
             pltpu.VMEM((slab_rows, blocks, HALF_COLS, 2 * inner), bf16),
+            pltpu.VMEM((WIN_ROWS * slab_cols, 2 * inner), bf16),
             pltpu.VMEM((tokens, inner), bf16),
             pltpu.VMEM((tokens, model_width), f32),
             pltpu.VMEM((heads, tokens, HEAD_DIM), f32),

time: 16.4 us -> 16.4 us (level)
  no operation moved by 1% of the time
where the time goes in v6:
time: 16.4 us; the launch traced here: 16.2 us
  Pallas kernels  15.5 us (95%)
  local copies, waits for them, and re-layouts  0.71 us (4%)
    pallas_call x1, Pallas kernels, on_device(): pl.pallas_call(functools.partial(kernel, sp_count=sp_count, tp_count=tp_c...  15.5 us
    unnamed x1, local copies, waits for them, and re-layouts  0.71 us

profile of v6, /device:TPU:1, one launch (start us, length us, event | category | flops | bytes accessed | tf_op | source)
XLA Modules:
  0.0 16.2 jit_solution(966762892391237396)
XLA Ops:
  0.0 15.5 %shard_map.73 = bf16[8,16,1024]{2,1,0:T(8,128)(2,1)S(1)} custom-call(bf16[8,2,8,1024]{3,2,1,0:T(8,128)(2,1)} %bitcast.2, f32[2,1024]{1,0:T(2,128)} %gain_hbm.1, bf16[2,1024,512]{2,1,0:T(8,128)(2,1)} %wq_hbm.1, bf16[2,1024,512]{2,1,0:T(8,128)(2,1)} %wk_hbm.1, bf16[2,1024,512]{2,1,0:T(8,128)(2,1)} %wv_hbm.1, f32[2,15,4,31]{3,2,1,0:T(4,128)} %bitcast.3, ...), custom_call_target="tpu_custom_call" | custom-call | tf_op jit(solution)/shard_map/pallas_call | solution.py:452
  15.5 0.7 %copy.9 = bf16[8,16,1024]{2,1,0:T(8,128)(2,1)} copy(bf16[8,16,1024]{2,1,0:T(8,128)(2,1)S(1)} %shard_map.73) | data formatting | bytes 524288

commit v7 on v5

--- a/solution.py
+++ b/solution.py
@@ -93,7 +93,8 @@
     def fetch(l, names):
         for name in names:
             src, dst = pairs[name]
-            copy = pltpu.make_async_copy(src.at[l], dst.at[l], w_sem.at[l, "kvqo".index(name)])
+            done = local_sem.at[0] if (l, name) == (0, "o") else w_sem.at[max(l - 1, 0), "kvqo".index(name)]
+            copy = pltpu.make_async_copy(src.at[l], dst.at[l], done)
             copy.start()
             weight_copies[l, name] = copy
 
@@ -358,13 +359,13 @@
                 device_id_type=MESH,
             )
     fetch(0, "o")
-    for later in range(1, layers):
-        fetch(later, "kvqo")
     first[1].wait()
     acc[...] = gather(xs, OWN)
     for l in range(layers):
         if l == 0:
             arrived(0, "kvq")
+            for later in range(1, layers):
+                fetch(later, "kvqo")
             send(0, OUTER)
         prepare_own(l)
         if l == 0:
@@ -473,7 +474,7 @@
             pltpu.VMEM((heads, tokens, HEAD_DIM), f32),
             pltpu.VMEM((heads, tokens, 2 * HEAD_DIM), f32),
             pltpu.SemaphoreType.DMA((3,)),
-            pltpu.SemaphoreType.DMA((layers, 4)),
+            pltpu.SemaphoreType.DMA((max(layers - 1, 1), 4)),
             pltpu.SemaphoreType.DMA((len(KINDS),)),
             pltpu.SemaphoreType.DMA((layers, len(KINDS))),
             pltpu.SemaphoreType.REGULAR((2,)),

time: 16.4 us -> 16.3 us (level)
  no operation moved by 1% of the time
where the time goes in v7:
time: 16.3 us; the launch traced here: 16.2 us
  Pallas kernels  15.4 us (94%)
  local copies, waits for them, and re-layouts  0.71 us (4%)
    pallas_call x1, Pallas kernels, on_device(): pl.pallas_call(functools.partial(kernel, sp_count=sp_count, tp_count=tp_c...  15.4 us
    unnamed x1, local copies, waits for them, and re-layouts  0.71 us

profile of v7, /device:TPU:1, one launch (start us, length us, event | category | flops | bytes accessed | tf_op | source)
XLA Modules:
  0.0 16.2 jit_solution(11838167415837528646)
XLA Ops:
  0.0 15.4 %shard_map.73 = bf16[8,16,1024]{2,1,0:T(8,128)(2,1)S(1)} custom-call(bf16[8,2,8,1024]{3,2,1,0:T(8,128)(2,1)} %bitcast.2, f32[2,1024]{1,0:T(2,128)} %gain_hbm.1, bf16[2,1024,512]{2,1,0:T(8,128)(2,1)} %wq_hbm.1, bf16[2,1024,512]{2,1,0:T(8,128)(2,1)} %wk_hbm.1, bf16[2,1024,512]{2,1,0:T(8,128)(2,1)} %wv_hbm.1, f32[2,15,4,31]{3,2,1,0:T(4,128)} %bitcast.3, ...), custom_call_target="tpu_custom_call" | custom-call | tf_op jit(solution)/shard_map/pallas_call | solution.py:453
  15.4 0.7 %copy.9 = bf16[8,16,1024]{2,1,0:T(8,128)(2,1)} copy(bf16[8,16,1024]{2,1,0:T(8,128)(2,1)S(1)} %shard_map.73) | data formatting | bytes 524288
